TPU v7x, 32 devices: a whole 2x2x4 slice. The times are simulated.
32 devices in a mesh: sp: 8 (over z, y), tp: 4 (over x, core).
Axes of the slice: x: 2, y: 2, z: 4, core: 2. Of those that a mesh axis runs over, the one named last changes fastest.
Arguments:
- residual_in: bfloat16 [6144, 2048], P('sp', 'tp'), may hold values from -11 to 11
- queries: bfloat16 [6144, 1024], P('sp', 'tp'), may hold values from -6 to 6
- keys: bfloat16 [6144, 256], P('sp'), may hold values from -6 to 6
- values: bfloat16 [6144, 256], P('sp'), may hold values from -6 to 6
- query_gain: float32 [128], replicated, may hold values from 1.5 to 5
- key_norm_gain: float32 [128], replicated, may hold values from 1.5 to 5
- out_weight: bfloat16 [1024, 2048], P('tp'), may hold values from -0.1875 to 0.1875
- mlp_gain: float32 [2048], replicated, may hold values from 0.1 to 1.9
- gate_weight: bfloat16 [2048, 5632], P('sp', 'tp'), may hold values from -0.125 to 0.125
- up_weight: bfloat16 [2048, 5632], P('sp', 'tp'), may hold values from -0.125 to 0.125
- down_weight: bfloat16 [5632, 2048], P('tp', 'sp'), may hold values from -0.15625 to 0.15625
Outputs:
- layer_out: bfloat16 [6144, 2048], P('sp', 'tp')
All inputs are finite; a program needn't handle non-finite values.
Results may differ from a plain program's by a relative error of at most 0.012.
The roundings to bfloat16 on the way count: a program that leaves them out, or rounds other values in their place, can miss the bound.
Values may be sent and summed in bfloat16 or wider, within the bound.
No kernel may reach another device: no remote copies, remote signals or barrier semaphores. Data moves between devices by JAX's collectives and lax.ppermute only.
A program may use at most 64 MiB of HBM per device.

v0:
```python
import jax
import jax.numpy as jnp
from jax import lax
from jax.sharding import PartitionSpec as P

D = 2048
HEAD_SIZE = 128
QUERY_HEADS = 8
KEY_VALUE_HEADS = 2
GRID = 64
eps = 1e-06
rotary_base = 10000.0


def apply_rotary(vectors, grid_positions):
    half_size = vectors.shape[-1] // 2
    frequency = rotary_base ** (-jnp.arange(0, half_size, 2, dtype=jnp.float32) / half_size)
    grid_row = (grid_positions // GRID).astype(jnp.float32)
    grid_col = (grid_positions % GRID).astype(jnp.float32)
    angles = jnp.concatenate(
        [grid_row[:, None] * frequency, grid_col[:, None] * frequency], axis=-1
    )[:, None, :]
    cosine_table = jnp.cos(angles)
    sine_table = jnp.sin(angles)
    first_half = vectors[..., :half_size]
    second_half = vectors[..., half_size:]
    return jnp.concatenate(
        [
            first_half * cosine_table - second_half * sine_table,
            first_half * sine_table + second_half * cosine_table,
        ],
        axis=-1,
    )


def per_head_norm(vectors, gain):
    return vectors * lax.rsqrt(jnp.mean(vectors * vectors, axis=-1, keepdims=True) + eps) * gain


def on_device(
    residual_in,
    queries,
    keys,
    values,
    query_gain,
    key_norm_gain,
    out_weight,
    mlp_gain,
    gate_weight,
    up_weight,
    down_weight,
):
    local_rows = residual_in.shape[0]
    local_heads = queries.shape[1] // HEAD_SIZE
    queries_per_group = QUERY_HEADS // KEY_VALUE_HEADS
    tp_index = lax.axis_index("tp")
    grid_positions = lax.axis_index("sp") * local_rows + jnp.arange(local_rows, dtype=jnp.int32)
    query_rows = apply_rotary(
        per_head_norm(
            queries.astype(jnp.float32).reshape(local_rows, local_heads, HEAD_SIZE), query_gain
        ),
        grid_positions,
    ).astype(jnp.bfloat16)
    query_matrix = jnp.transpose(query_rows, (1, 0, 2)).reshape(local_heads * local_rows, HEAD_SIZE)
    shared = tp_index * local_heads // queries_per_group
    own_keys = lax.dynamic_slice_in_dim(keys, shared * HEAD_SIZE, HEAD_SIZE, 1)
    own_values = lax.dynamic_slice_in_dim(values, shared * HEAD_SIZE, HEAD_SIZE, 1)
    key_matrix = apply_rotary(
        per_head_norm(own_keys.astype(jnp.float32)[:, None, :], key_norm_gain), grid_positions
    )[:, 0, :].astype(jnp.bfloat16)
    score_scale = HEAD_SIZE ** (-0.5)
    query_count = local_heads * local_rows
    start_state = (
        jnp.full((query_count,), -1e30, jnp.float32),
        jnp.zeros((query_count,), jnp.float32),
        jnp.zeros((query_count, HEAD_SIZE), jnp.float32),
    )
    key_piece = lax.all_gather(key_matrix, "sp", axis=0, tiled=True)
    value_piece = lax.all_gather(own_values, "sp", axis=0, tiled=True)
    piece_rows = key_piece.shape[0]
    block_count = -(-piece_rows // 2048)
    while piece_rows % block_count:
        block_count += 1
    block_width = piece_rows // block_count

    def one_block(block_index, state_inner):
        running_max, running_sum, weighted = state_inner
        block_keys = lax.dynamic_slice_in_dim(key_piece, block_index * block_width, block_width, 0)
        block_values = lax.dynamic_slice_in_dim(
            value_piece, block_index * block_width, block_width, 0
        )
        scores = (
            jnp.dot(query_matrix, block_keys.T, preferred_element_type=jnp.float32) * score_scale
        )
        new_max = jnp.maximum(running_max, jnp.max(scores, axis=1))
        factor = jnp.exp(running_max - new_max)
        weights = jnp.exp(scores - new_max[:, None])
        running_sum = running_sum * factor + jnp.sum(weights, axis=1)
        weighted = weighted * factor[:, None] + jnp.dot(
            weights.astype(jnp.bfloat16), block_values, preferred_element_type=jnp.float32
        )
        return (new_max, running_sum, weighted)

    running_max, running_sum, weighted = lax.fori_loop(0, block_count, one_block, start_state)
    attended = (weighted / running_sum[:, None]).astype(jnp.bfloat16)
    attended = jnp.transpose(
        attended.reshape(local_heads, local_rows, HEAD_SIZE), (1, 0, 2)
    ).reshape(local_rows, local_heads * HEAD_SIZE)
    own_width = residual_in.shape[1]
    projected = jnp.dot(attended, out_weight, preferred_element_type=jnp.float32).astype(
        jnp.bfloat16
    )
    share = lax.psum_scatter(projected, "tp", scatter_dimension=1, tiled=True).astype(jnp.float32)
    residual_mid = residual_in.astype(jnp.float32) + share
    squares = lax.psum(jnp.sum(residual_mid * residual_mid, axis=1), "tp")
    gain_own = lax.dynamic_slice_in_dim(mlp_gain, tp_index * own_width, own_width, 0)
    normed_own = (residual_mid * lax.rsqrt(squares / D + eps)[:, None] * gain_own).astype(
        jnp.bfloat16
    )
    normed = lax.all_gather(normed_own, "tp", axis=1, tiled=True)
    gate_out = jnp.dot(
        normed,
        lax.all_gather(gate_weight, "sp", axis=0, tiled=True),
        preferred_element_type=jnp.float32,
    )
    up_out = jnp.dot(
        normed,
        lax.all_gather(up_weight, "sp", axis=0, tiled=True),
        preferred_element_type=jnp.float32,
    )
    hidden = (jax.nn.silu(gate_out) * up_out).astype(jnp.bfloat16)
    down_terms = jnp.dot(
        hidden,
        lax.all_gather(down_weight, "sp", axis=1, tiled=True),
        preferred_element_type=jnp.float32,
    )
    down_share = lax.psum_scatter(
        down_terms.astype(jnp.bfloat16), "tp", scatter_dimension=1, tiled=True
    ).astype(jnp.float32)
    return (residual_mid + 0.5 * down_share).astype(jnp.bfloat16)


def solution(mesh):
    in_specs = (
        P("sp", "tp"),
        P("sp", "tp"),
        P("sp", None),
        P("sp", None),
        P(),
        P(),
        P("tp", None),
        P(),
        P("sp", "tp"),
        P("sp", "tp"),
        P("tp", "sp"),
    )
    out_specs = P("sp", "tp")
    return jax.shard_map(
        on_device, mesh=mesh, in_specs=in_specs, out_specs=out_specs, check_vma=False
    )
```

profile of v0, /device:TPU:0, one launch (start us, length us, event | category | flops | bytes accessed | tf_op | source)
XLA Modules:
  0.0 573.1 jit_solution(10254005252952721331)
XLA Ops:
  9.2 1.8 subtract_convert_fusion.1
  12.8 1.4 reshape.236
  14.1 1.7 fusion.18
  17.8 1.4 subtract_convert_fusion
  20.3 38.6 %all-gather.18.cloned.1.call-done = bf16[6144,1,128]{2,0,1:T(8,128)(2,1)} async-done(((bf16[768,1,128]{2,0,1:T(8,128)(2,1)}), bf16[6144,1,128]{2,0,1:T(8,128)(2,1)}) %all-gather.18.cloned.1.call-update) | async-done | bytes 1572880 | tf_op jit(solution)/shard_map/all_gather | solution.py:78
  58.9 44.8 %all-gather.8.cloned.1.call-done = bf16[6144,128]{1,0:T(8,128)(2,1)} async-done(((bf16[768,128]{1,0:T(8,128)(2,1)}), bf16[6144,128]{1,0:T(8,128)(2,1)}) %all-gather.8.cloned.1.call-update) | async-done | bytes 1572880 | tf_op jit(solution)/shard_map/all_gather | solution.py:79
  103.7 57.6 %while.18 = (s32[]{:T(128)}, f32[1536]{0:T(1024)S(1)}, f32[1536]{0:T(1024)S(1)}, f32[1536,128]{1,0:T(8,128)S(1)}, bf16[6144,128]{1,0:T(8,128)(2,1)}, /*index=5*/...) while((s32[]{:T(128)}, f32[1536]{0:T(1024)S(1)}, ...), condition=%wide.region_5.6_spmd.clone, body=%wide.region_2.5_spmd.clone.sunk | while | flops 1636376064 | bytes 91193544 | solution.py:104
  103.7 7.4 %multiply_reduce_fusion.4 = (f32[1536]{0:T(1024)S(1)}, f32[2048,1536]{1,0:T(8,128)}) fusion(bf16[1536,128]{1,0:T(8,128)(2,1)S(1)} %get-tuple-element.266, bf16[6144,128]{1,0:T(8,128)(2,1)} %get-tuple-element.265, s32[]{:T(128)S(6)} %select_n.55), kind=kOutput, calls=%fused_computation.1.clone.1 | convolution fusion | flops 811596288 | bytes 13506564 | tf_op jit(solution)/shard_map/while/body/eval_jaxpr/dot_general | solution.py:93
  111.1 6.8 %fusion.49 = f32[1536]{0:T(1024)S(1)} fusion(f32[2048,1536]{1,0:T(8,128)} %get-tuple-element.236, f32[1536]{0:T(1024)S(1)} %select_maximum_fusion.2), kind=kLoop, calls=%fused_computation.3.clone.1 | loop fusion | flops 9435648 | bytes 12595200 | tf_op jit(solution)/shard_map/while/body/eval_jaxpr/reduce_sum | solution.py:98
  117.9 1.3 copy-done.1
  119.2 3.6 fusion.51
  122.9 7.4 %multiply_reduce_fusion.4 = (f32[1536]{0:T(1024)S(1)}, f32[2048,1536]{1,0:T(8,128)}) fusion(bf16[1536,128]{1,0:T(8,128)(2,1)S(1)} %get-tuple-element.266, bf16[6144,128]{1,0:T(8,128)(2,1)} %get-tuple-element.265, s32[]{:T(128)S(6)} %select_n.55), kind=kOutput, calls=%fused_computation.1.clone.1 | convolution fusion | flops 811596288 | bytes 13506564 | tf_op jit(solution)/shard_map/while/body/eval_jaxpr/dot_general | solution.py:93
  130.3 6.8 %fusion.49 = f32[1536]{0:T(1024)S(1)} fusion(f32[2048,1536]{1,0:T(8,128)} %get-tuple-element.236, f32[1536]{0:T(1024)S(1)} %select_maximum_fusion.2), kind=kLoop, calls=%fused_computation.3.clone.1 | loop fusion | flops 9435648 | bytes 12595200 | tf_op jit(solution)/shard_map/while/body/eval_jaxpr/reduce_sum | solution.py:98
  137.1 1.3 copy-done.1
  138.4 3.6 fusion.51
  142.1 7.4 %multiply_reduce_fusion.4 = (f32[1536]{0:T(1024)S(1)}, f32[2048,1536]{1,0:T(8,128)}) fusion(bf16[1536,128]{1,0:T(8,128)(2,1)S(1)} %get-tuple-element.266, bf16[6144,128]{1,0:T(8,128)(2,1)} %get-tuple-element.265, s32[]{:T(128)S(6)} %select_n.55), kind=kOutput, calls=%fused_computation.1.clone.1 | convolution fusion | flops 811596288 | bytes 13506564 | tf_op jit(solution)/shard_map/while/body/eval_jaxpr/dot_general | solution.py:93
  149.5 6.8 %fusion.49 = f32[1536]{0:T(1024)S(1)} fusion(f32[2048,1536]{1,0:T(8,128)} %get-tuple-element.236, f32[1536]{0:T(1024)S(1)} %select_maximum_fusion.2), kind=kLoop, calls=%fused_computation.3.clone.1 | loop fusion | flops 9435648 | bytes 12595200 | tf_op jit(solution)/shard_map/while/body/eval_jaxpr/reduce_sum | solution.py:98
  156.3 1.3 copy-done.1
  157.6 3.6 fusion.51
  161.8 2.7 convolution_convert_fusion
  166.1 34.7 %reduce-scatter.3.cloned.1.call-done = bf16[768,512]{1,0:T(8,128)(2,1)} async-done(((bf16[768,2048]{1,0:T(8,128)(2,1)}), bf16[768,512]{1,0:T(8,128)(2,1)}) %reduce-scatter.3.cloned.1.call-update) | async-done | bytes 786448 | tf_op jit(solution)/shard_map/reduce_scatter | solution.py:113
  200.8 1.5 multiply_reduce_fusion.1
  202.2 5.8 %psum.7 = f32[768]{0:T(1024)S(1)} all-reduce(f32[768]{0:T(1024)S(1)} %multiply_reduce_fusion.1), channel_id=1, replica_groups=mesh['sp'=8,'tp'=4] {'tp'}, use_global_device_ids=true, to_apply=%region_8.9 | all-reduce | flops 768 | bytes 6144 | tf_op jit(solution)/shard_map/psum | solution.py:115
  208.0 2.3 multiply_convert_fusion.1
  211.7 83.4 %all-gather.12.cloned.1.call-done = bf16[2048,1408]{1,0:T(8,128)(2,1)} async-done(((bf16[256,1408]{1,0:T(8,128)(2,1)}), bf16[2048,1408]{1,0:T(8,128)(2,1)}) %all-gather.12.cloned.1.call-update) | async-done | bytes 5767184 | tf_op jit(solution)/shard_map/all_gather | solution.py:123
  295.1 28.1 %all-gather.10.cloned.1.call-done = bf16[768,2048]{1,0:T(8,128)(2,1)} async-done(((bf16[768,512]{1,0:T(8,128)(2,1)}), bf16[768,2048]{1,0:T(8,128)(2,1)}) %all-gather.10.cloned.1.call-update) | async-done | bytes 3145744 | tf_op jit(solution)/shard_map/all_gather | solution.py:120
  323.3 9.7 %fusion.31 = f32[768,1408]{1,0:T(8,128)} fusion(bf16[768,2048]{1,0:T(8,128)(2,1)} %all-gather.10.cloned.1.call-done, bf16[2048,1408]{1,0:T(8,128)(2,1)} %all-gather.12.cloned.1.call-done), kind=kOutput, calls=%fused_computation.68 | convolution fusion | flops 4429185024 | bytes 13238272 | tf_op jit(solution)/shard_map/dot_general | solution.py:121
  333.0 84.7 %all-gather.14.cloned.1.call-done = bf16[2048,1408]{1,0:T(8,128)(2,1)} async-done(((bf16[256,1408]{1,0:T(8,128)(2,1)}), bf16[2048,1408]{1,0:T(8,128)(2,1)}) %all-gather.14.cloned.1.call-update) | async-done | bytes 5767184 | tf_op jit(solution)/shard_map/all_gather | solution.py:128
  417.6 93.4 %all-gather.16.cloned.1.call-done = bf16[1408,2048]{1,0:T(8,128)(2,1)} async-done(((bf16[1408,256]{1,0:T(8,128)(2,1)}), bf16[1408,2048]{1,0:T(8,128)(2,1)}) %all-gather.16.cloned.1.call-update) | async-done | bytes 5767184 | tf_op jit(solution)/shard_map/all_gather | solution.py:134
  511.0 16.8 %convolution_convert_fusion.1 = bf16[768,2048]{1,0:T(8,128)(2,1)} fusion(bf16[1408,2048]{1,0:T(8,128)(2,1)} %all-gather.16.cloned.1.call-done, f32[768,1408]{1,0:T(8,128)} %fusion.31, bf16[768,2048]{1,0:T(8,128)(2,1)} %all-gather.10.cloned.1.call-done, bf16[2048,1408]{1,0:T(8,128)(2,1)} %all-gather.14.cloned.1.call-done), kind=kOutput, calls=%fused_computation.19 | convolution fusion | flops 8866430976 | bytes 22151168 | tf_op jit(solution)/shard_map/dot_general | solution.py:132
  527.8 36.1 %reduce-scatter.5.cloned.1.call-done = bf16[768,512]{1,0:T(8,128)(2,1)} async-done(((bf16[768,2048]{1,0:T(8,128)(2,1)}), bf16[768,512]{1,0:T(8,128)(2,1)}) %reduce-scatter.5.cloned.1.call-update) | async-done | bytes 786448 | tf_op jit(solution)/shard_map/reduce_scatter | solution.py:137
  563.9 2.3 add_convert_fusion
  (58 shorter events, 10.8 us)
Async XLA Ops:
  6.5 155.2 %copy-start = (bf16[256,2048]{1,0:T(8,128)(2,1)S(1)}, bf16[256,2048]{1,0:T(8,128)(2,1)}, u32[]{:S(2)}) copy-start(bf16[256,2048]{1,0:T(8,128)(2,1)} %param.19) | copy-start | bytes 3145732
  6.5 5.4 copy-start.4
  6.5 52.4 %all-gather.18.cloned.1.call-start = ((), (), s32[]{:S(2)}) async-start(), calls=%async_computation.9 | async-start | bytes 1769472 | tf_op jit(solution)/shard_map/all_gather | solution.py:78
  9.2 7.5 %copy-start.5 = (f32[128]{0:T(128)S(1)}, f32[128]{0:T(128)}, u32[]{:S(2)}) copy-start(f32[128]{0:T(128)} %param.17) | copy-start | bytes 1540
  11.9 91.8 %all-gather.8.cloned.1.call-start = ((), (), s32[]{:S(2)}) async-start(), calls=%async_computation.2 | async-start | bytes 1769472 | tf_op jit(solution)/shard_map/all_gather | solution.py:79
  12.7 188.1 %reduce-scatter.3.cloned.1.call-start = ((), (), s32[]{:S(2)}) async-start(), calls=%async_computation.3 | async-start | bytes 3932160 | tf_op jit(solution)/shard_map/reduce_scatter | solution.py:113
  111.1 8.2 %copy-start.1 = (f32[2048,1536]{1,0:T(8,128)S(1)}, f32[2048,1536]{1,0:T(8,128)}, u32[]{:S(2)}) copy-start(f32[2048,1536]{1,0:T(8,128)} %get-tuple-element.236) | copy-start | bytes 37748740 | tf_op jit(solution)/shard_map/while
  130.3 8.2 %copy-start.1 = (f32[2048,1536]{1,0:T(8,128)S(1)}, f32[2048,1536]{1,0:T(8,128)}, u32[]{:S(2)}) copy-start(f32[2048,1536]{1,0:T(8,128)} %get-tuple-element.236) | copy-start | bytes 37748740 | tf_op jit(solution)/shard_map/while
  149.5 8.2 %copy-start.1 = (f32[2048,1536]{1,0:T(8,128)S(1)}, f32[2048,1536]{1,0:T(8,128)}, u32[]{:S(2)}) copy-start(f32[2048,1536]{1,0:T(8,128)} %get-tuple-element.236) | copy-start | bytes 37748740 | tf_op jit(solution)/shard_map/while
  161.8 39.0 %copy-start.2 = (bf16[768,512]{1,0:T(8,128)(2,1)S(1)}, bf16[768,512]{1,0:T(8,128)(2,1)}, u32[]{:S(2)}) copy-start(bf16[768,512]{1,0:T(8,128)(2,1)} %param.13) | copy-start | bytes 2359300
  164.5 130.6 %all-gather.12.cloned.1.call-start = ((), (), s32[]{:S(2)}) async-start(), calls=%async_computation.5 | async-start | bytes 6488064 | tf_op jit(solution)/shard_map/all_gather | solution.py:123
  165.1 158.2 %all-gather.10.cloned.1.call-start = ((), (), s32[]{:S(2)}) async-start(), calls=%async_computation.4 | async-start | bytes 3932160 | tf_op jit(solution)/shard_map/all_gather | solution.py:120
  210.3 207.3 %all-gather.14.cloned.1.call-start = ((), (), s32[]{:S(2)}) async-start(), calls=%async_computation.6 | async-start | bytes 6488064 | tf_op jit(solution)/shard_map/all_gather | solution.py:128
  210.9 300.1 %all-gather.16.cloned.1.call-start = ((), (), s32[]{:S(2)}) async-start(), calls=%async_computation.7 | async-start | bytes 6488064 | tf_op jit(solution)/shard_map/all_gather | solution.py:134
  211.7 352.2 %reduce-scatter.5.cloned.1.call-start = ((), (), s32[]{:S(2)}) async-start(), calls=%async_computation.8 | async-start | bytes 3932160 | tf_op jit(solution)/shard_map/reduce_scatter | solution.py:137
  333.0 230.9 %copy-start.3 = (bf16[768,512]{1,0:T(8,128)(2,1)S(1)}, bf16[768,512]{1,0:T(8,128)(2,1)}, u32[]{:S(2)}) copy-start(bf16[768,512]{1,0:T(8,128)(2,1)} %reduce-scatter.3.cloned.1.call-done) | copy-start | bytes 2359300
Sparse Core Ops, SparseCore 0:
  12.0 46.8 all-gather.17
  61.1 42.5 all-gather.7
  164.6 36.0 reduce-scatter.2
  202.8 92.2 all-gather.11
  296.5 26.6 all-gather.9
  325.3 92.3 all-gather.13
  419.7 91.2 all-gather.15
  527.9 35.8 reduce-scatter.4
where the time goes:
time: 574 us; the launch traced here: 573 us
  waiting for transfers between devices  446 us (78%)
  matrix products  62.2 us (11%)
  other arithmetic  38.3 us (7%)
  between operations  13.7 us (2%)
  local copies, waits for them, and re-layouts  7.03 us (1%)
  blocking collectives  5.77 us (1%)
    all_gather x1, waiting for transfers between devices, on_device(): lax.all_gather(down_weight, 'sp', axis=1, tiled=True)  93.4 us
    all_gather x1, waiting for transfers between devices, on_device(): lax.all_gather(up_weight, 'sp', axis=0, tiled=True)  84.7 us
    all_gather x1, waiting for transfers between devices, on_device(): lax.all_gather(gate_weight, 'sp', axis=0, tiled=True)  83.4 us
    all_gather x1, waiting for transfers between devices, on_device(): value_piece = lax.all_gather(own_values, 'sp', axis=0, tiled=True)  44.8 us
    all_gather x1, waiting for transfers between devices, on_device(): key_piece = lax.all_gather(key_matrix, 'sp', axis=0, tiled=True)  38.6 us
    reduce_scatter x1, waiting for transfers between devices, on_device(): lax.psum_scatter(down_terms.astype(jnp.bfloat16), 'tp', scatter_dimension...  36.1 us
    reduce_scatter x1, waiting for transfers between devices, on_device(): lax.psum_scatter(projected, 'tp', scatter_dimension=1, tiled=True)  34.7 us
    all_gather x1, waiting for transfers between devices, on_device(): normed = lax.all_gather(normed_own, 'tp', axis=1, tiled=True)  28.1 us
  transfers between devices with their start and end apart: 8, of which 8 were waited for; matrix products, arithmetic and copies ran while one was open for 4% of the time, Pallas kernels for 0%

commit v1 on v0

--- a/solution.py
+++ b/solution.py
@@ -10,6 +10,17 @@
 GRID = 64
 eps = 1e-06
 rotary_base = 10000.0
+
+
+def gather_by_hops(shard, name, dim):
+    n_dev = lax.axis_size(name)
+    right = [(i, (i + 1) % n_dev) for i in range(n_dev)]
+    terms = [shard]
+    for reach in range(1, n_dev):
+        terms = [lax.ppermute(terms[0], name, right), *terms]
+    whole = jnp.concatenate(terms, axis=dim)
+    turn = (lax.axis_index(name) + 1) * terms[-1].shape[dim]
+    return jnp.roll(whole, turn, axis=dim)
 
 
 def apply_rotary(vectors, grid_positions):
@@ -76,7 +87,7 @@
         jnp.zeros((query_count, HEAD_SIZE), jnp.float32),
     )
     key_piece = lax.all_gather(key_matrix, "sp", axis=0, tiled=True)
-    value_piece = lax.all_gather(own_values, "sp", axis=0, tiled=True)
+    value_piece = gather_by_hops(own_values, "sp", 0)
     piece_rows = key_piece.shape[0]
     block_count = -(-piece_rows // 2048)
     while piece_rows % block_count:

time: 574 us -> 556 us (0.969)
  waiting for transfers between devices: 446 us -> 416 us
  local copies, waits for them, and re-layouts: 7.03 us -> 15.9 us
    ppermute x0 -> x7, waiting for transfers between devices: none -> 50.2 us  [gather_by_hops(): terms = [lax.ppermute(terms[0], name, right), *terms]]
    all_gather x1 -> x0, waiting for transfers between devices: 44.8 us -> none  [on_device(): value_piece = lax.all_gather(own_values, 'sp', axis=0, tiled=True)]
    all_gather x1, waiting for transfers between devices: 38.6 us -> 2.89 us  [on_device(): key_piece = lax.all_gather(key_matrix, 'sp', axis=0, tiled=True)]
    unnamed x10 -> x37, local copies, waits for them, and re-layouts: 0.02 us -> 6.96 us
  transfers between devices with their start and end apart: 8 -> 14, of which waited for: 8 -> 14; matrix products, arithmetic and copies ran while one was open for 4% -> 6% of each run, Pallas kernels for 0% -> 0%
where the time goes in v1:
time: 556 us; the launch traced here: 555 us
  waiting for transfers between devices  416 us (75%)
  matrix products  62.2 us (11%)
  other arithmetic  38.1 us (7%)
  local copies, waits for them, and re-layouts  15.9 us (3%)
  between operations  13.9 us (2%)
  blocking collectives  5.77 us (1%)
    all_gather x1, waiting for transfers between devices, on_device(): lax.all_gather(down_weight, 'sp', axis=1, tiled=True)  93.2 us
    all_gather x1, waiting for transfers between devices, on_device(): lax.all_gather(up_weight, 'sp', axis=0, tiled=True)  84.7 us
    all_gather x1, waiting for transfers between devices, on_device(): lax.all_gather(gate_weight, 'sp', axis=0, tiled=True)  83.5 us
    ppermute x7, waiting for transfers between devices, gather_by_hops(): terms = [lax.ppermute(terms[0], name, right), *terms]  50.2 us
    reduce_scatter x1, waiting for transfers between devices, on_device(): lax.psum_scatter(down_terms.astype(jnp.bfloat16), 'tp', scatter_dimension...  36.1 us
    reduce_scatter x1, waiting for transfers between devices, on_device(): lax.psum_scatter(projected, 'tp', scatter_dimension=1, tiled=True)  35.1 us
    all_gather x1, waiting for transfers between devices, on_device(): normed = lax.all_gather(normed_own, 'tp', axis=1, tiled=True)  28.1 us
    dot_general x3, matrix products, one_block(): jnp.dot(query_matrix, block_keys.T, preferred_element_type=jnp.float32)  22.1 us
  transfers between devices with their start and end apart: 14, of which 14 were waited for; matrix products, arithmetic and copies ran while one was open for 6% of the time, Pallas kernels for 0%

profile of v1, /device:TPU:0, one launch (start us, length us, event | category | flops | bytes accessed | tf_op | source)
XLA Modules:
  0.0 555.0 jit_solution(7359884262307826526)
XLA Ops:
  7.6 3.0 collective-permute-start
  12.1 6.5 %collective-permute-done = bf16[768,128]{1,0:T(8,128)(2,1)S(1)} collective-permute-done((bf16[768,128]{1,0:T(8,128)(2,1)S(1)}, bf16[768,128]{1,0:T(8,128)(2,1)S(1)}, u32[]{:S(2)}, u32[]{:S(2)}) %collective-permute-start) | collective-permute-done | bytes 196640 | tf_op jit(solution)/shard_map/ppermute | solution.py:20
  19.7 7.6 %collective-permute-done.1 = bf16[768,128]{1,0:T(8,128)(2,1)S(1)} collective-permute-done((bf16[768,128]{1,0:T(8,128)(2,1)S(1)}, bf16[768,128]{1,0:T(8,128)(2,1)S(1)}, u32[]{:S(2)}, u32[]{:S(2)}) %collective-permute-start.1) | collective-permute-done | bytes 196640 | tf_op jit(solution)/shard_map/ppermute | solution.py:20
  27.3 1.8 subtract_convert_fusion.1
  29.1 6.6 %collective-permute-done.2 = bf16[768,128]{1,0:T(8,128)(2,1)S(1)} collective-permute-done((bf16[768,128]{1,0:T(8,128)(2,1)S(1)}, bf16[768,128]{1,0:T(8,128)(2,1)S(1)}, u32[]{:S(2)}, u32[]{:S(2)}) %collective-permute-start.2) | collective-permute-done | bytes 196640 | tf_op jit(solution)/shard_map/ppermute | solution.py:20
  38.8 5.2 collective-permute-done.3
  44.1 10.8 %collective-permute-done.4 = bf16[768,128]{1,0:T(8,128)(2,1)S(1)} collective-permute-done((bf16[768,128]{1,0:T(8,128)(2,1)S(1)}, bf16[768,128]{1,0:T(8,128)(2,1)S(1)}, u32[]{:S(2)}, u32[]{:S(2)}) %collective-permute-start.4) | collective-permute-done | bytes 196640 | tf_op jit(solution)/shard_map/ppermute | solution.py:20
  57.6 5.9 %collective-permute-done.5 = bf16[768,128]{1,0:T(8,128)(2,1)} collective-permute-done((bf16[768,128]{1,0:T(8,128)(2,1)S(1)}, bf16[768,128]{1,0:T(8,128)(2,1)}, u32[]{:S(2)}, u32[]{:S(2)}) %collective-permute-start.5) | collective-permute-done | bytes 196640 | tf_op jit(solution)/shard_map/ppermute | solution.py:20
  66.2 7.5 %collective-permute-done.6 = bf16[768,128]{1,0:T(8,128)(2,1)} collective-permute-done((bf16[768,128]{1,0:T(8,128)(2,1)}, bf16[768,128]{1,0:T(8,128)(2,1)}, u32[]{:S(2)}, u32[]{:S(2)}) %collective-permute-start.6) | collective-permute-done | bytes 196640 | tf_op jit(solution)/shard_map/ppermute | solution.py:20
  82.4 2.9 all-gather.15.cloned.1.call-done
  85.3 57.5 %while.18 = (s32[]{:T(128)}, f32[1536]{0:T(1024)S(1)}, f32[1536]{0:T(1024)S(1)}, f32[1536,128]{1,0:T(8,128)S(1)}, bf16[6144,128]{1,0:T(8,128)(2,1)}, /*index=5*/...) while((s32[]{:T(128)}, f32[1536]{0:T(1024)S(1)}, ...), condition=%wide.region_5.6_spmd.clone, body=%wide.region_2.5_spmd.clone.sunk | while | flops 1636376064 | bytes 91193544 | solution.py:115
  85.3 7.4 %multiply_reduce_fusion.4 = (f32[1536]{0:T(1024)S(1)}, f32[2048,1536]{1,0:T(8,128)}) fusion(bf16[1536,128]{1,0:T(8,128)(2,1)S(1)} %get-tuple-element.266, bf16[6144,128]{1,0:T(8,128)(2,1)} %get-tuple-element.265, s32[]{:T(128)S(6)} %select_n.69), kind=kOutput, calls=%fused_computation.1.clone.1 | convolution fusion | flops 811596288 | bytes 13506564 | tf_op jit(solution)/shard_map/while/body/eval_jaxpr/dot_general | solution.py:104
  92.6 6.8 %fusion.49 = f32[1536]{0:T(1024)S(1)} fusion(f32[2048,1536]{1,0:T(8,128)} %get-tuple-element.236, f32[1536]{0:T(1024)S(1)} %select_maximum_fusion.2), kind=kLoop, calls=%fused_computation.3.clone.1 | loop fusion | flops 9435648 | bytes 12595200 | tf_op jit(solution)/shard_map/while/body/eval_jaxpr/reduce_sum | solution.py:109
  100.8 3.6 fusion.51
  104.5 7.4 %multiply_reduce_fusion.4 = (f32[1536]{0:T(1024)S(1)}, f32[2048,1536]{1,0:T(8,128)}) fusion(bf16[1536,128]{1,0:T(8,128)(2,1)S(1)} %get-tuple-element.266, bf16[6144,128]{1,0:T(8,128)(2,1)} %get-tuple-element.265, s32[]{:T(128)S(6)} %select_n.69), kind=kOutput, calls=%fused_computation.1.clone.1 | convolution fusion | flops 811596288 | bytes 13506564 | tf_op jit(solution)/shard_map/while/body/eval_jaxpr/dot_general | solution.py:104
  111.8 6.8 %fusion.49 = f32[1536]{0:T(1024)S(1)} fusion(f32[2048,1536]{1,0:T(8,128)} %get-tuple-element.236, f32[1536]{0:T(1024)S(1)} %select_maximum_fusion.2), kind=kLoop, calls=%fused_computation.3.clone.1 | loop fusion | flops 9435648 | bytes 12595200 | tf_op jit(solution)/shard_map/while/body/eval_jaxpr/reduce_sum | solution.py:109
  120.0 3.6 fusion.51
  123.7 7.4 %multiply_reduce_fusion.4 = (f32[1536]{0:T(1024)S(1)}, f32[2048,1536]{1,0:T(8,128)}) fusion(bf16[1536,128]{1,0:T(8,128)(2,1)S(1)} %get-tuple-element.266, bf16[6144,128]{1,0:T(8,128)(2,1)} %get-tuple-element.265, s32[]{:T(128)S(6)} %select_n.69), kind=kOutput, calls=%fused_computation.1.clone.1 | convolution fusion | flops 811596288 | bytes 13506564 | tf_op jit(solution)/shard_map/while/body/eval_jaxpr/dot_general | solution.py:104
  131.0 6.8 %fusion.49 = f32[1536]{0:T(1024)S(1)} fusion(f32[2048,1536]{1,0:T(8,128)} %get-tuple-element.236, f32[1536]{0:T(1024)S(1)} %select_maximum_fusion.2), kind=kLoop, calls=%fused_computation.3.clone.1 | loop fusion | flops 9435648 | bytes 12595200 | tf_op jit(solution)/shard_map/while/body/eval_jaxpr/reduce_sum | solution.py:109
  139.2 3.6 fusion.51
  143.3 2.7 convolution_convert_fusion
  147.6 35.1 %reduce-scatter.3.cloned.1.call-done = bf16[768,512]{1,0:T(8,128)(2,1)} async-done(((bf16[768,2048]{1,0:T(8,128)(2,1)}), bf16[768,512]{1,0:T(8,128)(2,1)}) %reduce-scatter.3.cloned.1.call-update) | async-done | bytes 786448 | tf_op jit(solution)/shard_map/reduce_scatter | solution.py:124
  184.2 5.8 %psum.7 = f32[768]{0:T(1024)S(1)} all-reduce(f32[768]{0:T(1024)S(1)} %multiply_reduce_fusion.1), channel_id=1, replica_groups=mesh['sp'=8,'tp'=4] {'tp'}, use_global_device_ids=true, to_apply=%region_8.9 | all-reduce | flops 768 | bytes 6144 | tf_op jit(solution)/shard_map/psum | solution.py:126
  189.9 2.3 multiply_convert_fusion.1
  193.7 83.5 %all-gather.9.cloned.1.call-done = bf16[2048,1408]{1,0:T(8,128)(2,1)} async-done(((bf16[256,1408]{1,0:T(8,128)(2,1)}), bf16[2048,1408]{1,0:T(8,128)(2,1)}) %all-gather.9.cloned.1.call-update) | async-done | bytes 5767184 | tf_op jit(solution)/shard_map/all_gather | solution.py:134
  277.2 28.1 %all-gather.7.cloned.1.call-done = bf16[768,2048]{1,0:T(8,128)(2,1)} async-done(((bf16[768,512]{1,0:T(8,128)(2,1)}), bf16[768,2048]{1,0:T(8,128)(2,1)}) %all-gather.7.cloned.1.call-update) | async-done | bytes 3145744 | tf_op jit(solution)/shard_map/all_gather | solution.py:131
  305.4 9.7 %fusion.31 = f32[768,1408]{1,0:T(8,128)} fusion(bf16[768,2048]{1,0:T(8,128)(2,1)} %all-gather.7.cloned.1.call-done, bf16[2048,1408]{1,0:T(8,128)(2,1)} %all-gather.9.cloned.1.call-done), kind=kOutput, calls=%fused_computation.85 | convolution fusion | flops 4429185024 | bytes 13238272 | tf_op jit(solution)/shard_map/dot_general | solution.py:132
  315.1 84.7 %all-gather.11.cloned.1.call-done = bf16[2048,1408]{1,0:T(8,128)(2,1)} async-done(((bf16[256,1408]{1,0:T(8,128)(2,1)}), bf16[2048,1408]{1,0:T(8,128)(2,1)}) %all-gather.11.cloned.1.call-update) | async-done | bytes 5767184 | tf_op jit(solution)/shard_map/all_gather | solution.py:139
  399.7 93.2 %all-gather.13.cloned.1.call-done = bf16[1408,2048]{1,0:T(8,128)(2,1)} async-done(((bf16[1408,256]{1,0:T(8,128)(2,1)}), bf16[1408,2048]{1,0:T(8,128)(2,1)}) %all-gather.13.cloned.1.call-update) | async-done | bytes 5767184 | tf_op jit(solution)/shard_map/all_gather | solution.py:145
  493.0 16.8 %convolution_convert_fusion.1 = bf16[768,2048]{1,0:T(8,128)(2,1)} fusion(bf16[1408,2048]{1,0:T(8,128)(2,1)} %all-gather.13.cloned.1.call-done, f32[768,1408]{1,0:T(8,128)} %fusion.31, bf16[768,2048]{1,0:T(8,128)(2,1)} %all-gather.7.cloned.1.call-done, bf16[2048,1408]{1,0:T(8,128)(2,1)} %all-gather.11.cloned.1.call-done), kind=kOutput, calls=%fused_computation.19 | convolution fusion | flops 8866430976 | bytes 22151168 | tf_op jit(solution)/shard_map/dot_general | solution.py:143
  509.8 36.1 %reduce-scatter.5.cloned.1.call-done = bf16[768,512]{1,0:T(8,128)(2,1)} async-done(((bf16[768,2048]{1,0:T(8,128)(2,1)}), bf16[768,512]{1,0:T(8,128)(2,1)}) %reduce-scatter.5.cloned.1.call-update) | async-done | bytes 786448 | tf_op jit(solution)/shard_map/reduce_scatter | solution.py:148
  545.8 2.3 add_convert_fusion
  (98 shorter events, 29.3 us)
Async XLA Ops:
  6.5 136.8 %copy-start = (bf16[256,2048]{1,0:T(8,128)(2,1)S(1)}, bf16[256,2048]{1,0:T(8,128)(2,1)}, u32[]{:S(2)}) copy-start(bf16[256,2048]{1,0:T(8,128)(2,1)} %param.19) | copy-start | bytes 3145732
  6.5 78.7 %all-gather.15.cloned.1.call-start = ((), (), s32[]{:S(2)}) async-start(), calls=%async_computation.8 | async-start | bytes 1769472 | tf_op jit(solution)/shard_map/all_gather | solution.py:89
  7.6 11.0 %collective-permute-start = (bf16[768,128]{1,0:T(8,128)(2,1)S(1)}, bf16[768,128]{1,0:T(8,128)(2,1)S(1)}, u32[]{:S(2)}, u32[]{:S(2)}) collective-permute-start(bf16[768,128]{1,0:T(8,128)(2,1)S(1)} %constant_dynamic-slice_fusion.1), channel_id=1, source_target_pairs={{0,4},{4,8},{8,12},{12,16},{16,20},{20,24},{24,28},{28,0},{1,5},{5... | collective-permute-start | bytes 589832 | tf_op jit(solution)/shard_map/ppermute | solution.py:20
  12.1 42.9 %copy-start.11 = (f32[128]{0:T(128)S(1)}, f32[128]{0:T(128)}, u32[]{:S(2)}) copy-start(f32[128]{0:T(128)} %param.17) | copy-start | bytes 1540
  18.6 8.8 %collective-permute-start.1 = (bf16[768,128]{1,0:T(8,128)(2,1)S(1)}, bf16[768,128]{1,0:T(8,128)(2,1)S(1)}, u32[]{:S(2)}, u32[]{:S(2)}) collective-permute-start(bf16[768,128]{1,0:T(8,128)(2,1)S(1)} %collective-permute-done), channel_id=1, source_target_pairs={{0,4},{4,8},{8,12},{12,16},{16,20},{20,24},{24,28},{28,0},{1,5},{5... | collective-permute-start | bytes 589832 | tf_op jit(solution)/shard_map/ppermute | solution.py:20
  27.3 8.4 %collective-permute-start.2 = (bf16[768,128]{1,0:T(8,128)(2,1)S(1)}, bf16[768,128]{1,0:T(8,128)(2,1)S(1)}, u32[]{:S(2)}, u32[]{:S(2)}) collective-permute-start(bf16[768,128]{1,0:T(8,128)(2,1)S(1)} %collective-permute-done.1), channel_id=1, source_target_pairs={{0,4},{4,8},{8,12},{12,16},{16,20},{20,24},{24,28},{28,0},{1,5},{5... | collective-permute-start | bytes 589832 | tf_op jit(solution)/shard_map/ppermute | solution.py:20
  35.7 21.9 %copy-start.5 = (bf16[768,128]{1,0:T(8,128)(2,1)}, bf16[768,128]{1,0:T(8,128)(2,1)S(1)}, u32[]{:S(2)}) copy-start(bf16[768,128]{1,0:T(8,128)(2,1)S(1)} %collective-permute-done.2) | copy-start | bytes 589828
  35.7 8.4 %collective-permute-start.3 = (bf16[768,128]{1,0:T(8,128)(2,1)S(1)}, bf16[768,128]{1,0:T(8,128)(2,1)S(1)}, u32[]{:S(2)}, u32[]{:S(2)}) collective-permute-start(bf16[768,128]{1,0:T(8,128)(2,1)S(1)} %collective-permute-done.2), channel_id=1, source_target_pairs={{0,4},{4,8},{8,12},{12,16},{16,20},{20,24},{24,28},{28,0},{1,5},{5... | collective-permute-start | bytes 589832 | tf_op jit(solution)/shard_map/ppermute | solution.py:20
  36.5 146.2 %reduce-scatter.3.cloned.1.call-start = ((), (), s32[]{:S(2)}) async-start(), calls=%async_computation.2 | async-start | bytes 3932160 | tf_op jit(solution)/shard_map/reduce_scatter | solution.py:124
  44.1 19.5 %copy-start.7 = (bf16[768,128]{1,0:T(8,128)(2,1)}, bf16[768,128]{1,0:T(8,128)(2,1)S(1)}, u32[]{:S(2)}) copy-start(bf16[768,128]{1,0:T(8,128)(2,1)S(1)} %collective-permute-done.3) | copy-start | bytes 589828
  44.1 10.9 %collective-permute-start.4 = (bf16[768,128]{1,0:T(8,128)(2,1)S(1)}, bf16[768,128]{1,0:T(8,128)(2,1)S(1)}, u32[]{:S(2)}, u32[]{:S(2)}) collective-permute-start(bf16[768,128]{1,0:T(8,128)(2,1)S(1)} %collective-permute-done.3), channel_id=1, source_target_pairs={{0,4},{4,8},{8,12},{12,16},{16,20},{20,24},{24,28},{28,0},{1,5},{5... | collective-permute-start | bytes 589832 | tf_op jit(solution)/shard_map/ppermute | solution.py:20
  54.9 8.6 %copy-start.9 = (bf16[768,128]{1,0:T(8,128)(2,1)}, bf16[768,128]{1,0:T(8,128)(2,1)S(1)}, u32[]{:S(2)}) copy-start(bf16[768,128]{1,0:T(8,128)(2,1)S(1)} %collective-permute-done.4) | copy-start | bytes 589828
  54.9 8.6 %collective-permute-start.5 = (bf16[768,128]{1,0:T(8,128)(2,1)S(1)}, bf16[768,128]{1,0:T(8,128)(2,1)}, u32[]{:S(2)}, u32[]{:S(2)}) collective-permute-start(bf16[768,128]{1,0:T(8,128)(2,1)S(1)} %collective-permute-done.4), channel_id=1, source_target_pairs={{0,4},{4,8},{8,12},{12,16},{16,20},{20,24},{24,28},{28,0},{1,5},{5... | collective-permute-start | bytes 589832 | tf_op jit(solution)/shard_map/ppermute | solution.py:20
  63.5 10.2 %collective-permute-start.6 = (bf16[768,128]{1,0:T(8,128)(2,1)}, bf16[768,128]{1,0:T(8,128)(2,1)}, u32[]{:S(2)}, u32[]{:S(2)}) collective-permute-start(bf16[768,128]{1,0:T(8,128)(2,1)} %collective-permute-done.5), channel_id=1, source_target_pairs={{0,4},{4,8},{8,12},{12,16},{16,20},{20,24},{24,28},{28,0},{1,5},{5... | collective-permute-start | bytes 589832 | tf_op jit(solution)/shard_map/ppermute | solution.py:20
  64.9 13.6 %copy-start.4 = (bf16[768,256]{1,0:T(8,128)(2,1)S(1)}, bf16[768,256]{1,0:T(8,128)(2,1)}, u32[]{:S(2)}) copy-start(bf16[768,256]{1,0:T(8,128)(2,1)} %param.16) | copy-start | bytes 1179652
  66.1 14.5 %copy-start.8 = (bf16[768,128]{1,0:T(8,128)(2,1)S(1)}, bf16[768,128]{1,0:T(8,128)(2,1)}, u32[]{:S(2)}) copy-start(bf16[768,128]{1,0:T(8,128)(2,1)} %copy-done.7) | copy-start | bytes 589828
  66.1 14.6 %copy-start.6 = (bf16[768,128]{1,0:T(8,128)(2,1)S(1)}, bf16[768,128]{1,0:T(8,128)(2,1)}, u32[]{:S(2)}) copy-start(bf16[768,128]{1,0:T(8,128)(2,1)} %copy-done.5) | copy-start | bytes 589828
  66.2 14.4 %copy-start.10 = (bf16[768,128]{1,0:T(8,128)(2,1)S(1)}, bf16[768,128]{1,0:T(8,128)(2,1)}, u32[]{:S(2)}) copy-start(bf16[768,128]{1,0:T(8,128)(2,1)} %copy-done.9) | copy-start | bytes 589828
  92.6 8.2 %copy-start.1 = (f32[2048,1536]{1,0:T(8,128)S(1)}, f32[2048,1536]{1,0:T(8,128)}, u32[]{:S(2)}) copy-start(f32[2048,1536]{1,0:T(8,128)} %get-tuple-element.236) | copy-start | bytes 37748740 | tf_op jit(solution)/shard_map/while
  111.8 8.2 %copy-start.1 = (f32[2048,1536]{1,0:T(8,128)S(1)}, f32[2048,1536]{1,0:T(8,128)}, u32[]{:S(2)}) copy-start(f32[2048,1536]{1,0:T(8,128)} %get-tuple-element.236) | copy-start | bytes 37748740 | tf_op jit(solution)/shard_map/while
  131.0 8.2 %copy-start.1 = (f32[2048,1536]{1,0:T(8,128)S(1)}, f32[2048,1536]{1,0:T(8,128)}, u32[]{:S(2)}) copy-start(f32[2048,1536]{1,0:T(8,128)} %get-tuple-element.236) | copy-start | bytes 37748740 | tf_op jit(solution)/shard_map/while
  146.0 36.7 %copy-start.2 = (bf16[768,512]{1,0:T(8,128)(2,1)S(1)}, bf16[768,512]{1,0:T(8,128)(2,1)}, u32[]{:S(2)}) copy-start(bf16[768,512]{1,0:T(8,128)(2,1)} %param.13) | copy-start | bytes 2359300
  146.0 131.2 %all-gather.9.cloned.1.call-start = ((), (), s32[]{:S(2)}) async-start(), calls=%async_computation.4 | async-start | bytes 6488064 | tf_op jit(solution)/shard_map/all_gather | solution.py:134
  146.8 158.6 %all-gather.7.cloned.1.call-start = ((), (), s32[]{:S(2)}) async-start(), calls=%async_computation.3 | async-start | bytes 3932160 | tf_op jit(solution)/shard_map/all_gather | solution.py:131
  192.3 207.5 %all-gather.11.cloned.1.call-start = ((), (), s32[]{:S(2)}) async-start(), calls=%async_computation.5 | async-start | bytes 6488064 | tf_op jit(solution)/shard_map/all_gather | solution.py:139
  192.9 300.1 %all-gather.13.cloned.1.call-start = ((), (), s32[]{:S(2)}) async-start(), calls=%async_computation.6 | async-start | bytes 6488064 | tf_op jit(solution)/shard_map/all_gather | solution.py:145
  193.5 352.4 %reduce-scatter.5.cloned.1.call-start = ((), (), s32[]{:S(2)}) async-start(), calls=%async_computation.7 | async-start | bytes 3932160 | tf_op jit(solution)/shard_map/reduce_scatter | solution.py:148
  509.8 36.1 %copy-start.3 = (bf16[768,512]{1,0:T(8,128)(2,1)S(1)}, bf16[768,512]{1,0:T(8,128)(2,1)}, u32[]{:S(2)}) copy-start(bf16[768,512]{1,0:T(8,128)(2,1)} %reduce-scatter.3.cloned.1.call-done) | copy-start | bytes 2359300
Sparse Core Ops, SparseCore 0:
  36.6 48.5 all-gather.14
  146.2 36.4 reduce-scatter.2
  184.9 92.2 all-gather.8
  278.6 26.6 all-gather.6
  307.4 92.3 all-gather.10
  401.6 91.3 all-gather.12
  509.9 35.8 reduce-scatter.4
